TPU v7x, 32 devices: a whole 2x2x4 slice. The times are simulated.
32 devices in a mesh: kv: 8 (over z, x), tp: 4 (over y, core).
Axes of the slice: x: 2, y: 2, z: 4, core: 2. Of those that a mesh axis runs over, the one named last changes fastest.
Arguments:
- hidden: bfloat16 [128, 4, 2048], P(None, None, 'kv'), may hold values from -18 to 18
- norm_gain: float32 [2048], replicated, may hold values from 0.1 to 1.9
- w_query: bfloat16 [2048, 1024], P(None, 'tp'), may hold values from -0.125 to 0.125
- w_forget: bfloat16 [2048, 1024], P(None, 'tp'), may hold values from -0.125 to 0.125
- w_input: bfloat16 [2048, 1024], P(None, 'tp'), may hold values from -0.125 to 0.125
- w_outgate: bfloat16 [2048, 1024], P(None, 'tp'), may hold values from -0.125 to 0.125
- w_out: bfloat16 [1024, 2048], replicated, may hold values from -0.1875 to 0.1875
- floor: float32 [1024], P('tp'), may hold values from 0 to 0.95
- head_gain: float32 [128], replicated, may hold values from 0.1 to 1.9
- base_state: float32 [128, 8, 128, 128], P('kv', 'tp'), may hold values from -4 to 4
- prev_forget: bfloat16 [128, 4, 1024], P('kv', None, 'tp'), may hold values from -6 to 6
- prev_input: bfloat16 [128, 4, 1024], P('kv', None, 'tp'), may hold values from -6 to 6
- accepted: int32 [128], P('kv'), may hold values from 0 to 4
Outputs:
- mixed: bfloat16 [128, 4, 2048], P(None, None, 'kv')
- taken_state: float32 [128, 8, 128, 128], P('kv', 'tp')
All inputs are finite; a program needn't handle non-finite values.
Results may differ from a plain program's by a relative error of at most 0.014.
Values may be sent and summed in bfloat16 or wider, within the bound.
A program may use at most 64 MiB of HBM per device.

v0:
```python
import jax
import jax.numpy as jnp
from jax import lax
from jax.sharding import PartitionSpec as P

D = 2048
HEAD_DIM = 128
PROPS = 4


def shards(
    hidden,
    norm_gain,
    w_query,
    w_forget,
    w_input,
    w_outgate,
    w_out,
    floor,
    head_gain,
    base_state,
    prev_forget,
    prev_input,
    accepted,
):
    arrived = lax.all_to_all(hidden, "kv", split_axis=0, concat_axis=2, tiled=True)
    whole_vals = arrived.astype(jnp.float32)
    row_sums = jnp.sum(whole_vals * whole_vals, axis=2)
    normed = (whole_vals * lax.rsqrt(row_sums / D + 1e-06)[..., None] * norm_gain).astype(
        jnp.bfloat16
    )
    query_pre = jnp.dot(normed, w_query, preferred_element_type=jnp.float32).astype(jnp.bfloat16)
    forget_pre = jnp.dot(normed, w_forget, preferred_element_type=jnp.float32).astype(jnp.bfloat16)
    input_pre = jnp.dot(normed, w_input, preferred_element_type=jnp.float32).astype(jnp.bfloat16)
    gate_pre = jnp.dot(normed, w_outgate, preferred_element_type=jnp.float32).astype(jnp.bfloat16)
    seq_local = normed.shape[0]
    head_local = w_query.shape[1] // HEAD_DIM
    shape = (seq_local, PROPS, head_local, HEAD_DIM)
    query = jax.nn.silu(query_pre.astype(jnp.float32)).reshape(shape)
    forget = (floor + (1.0 - floor) * jax.nn.sigmoid(forget_pre.astype(jnp.float32))).reshape(shape)
    value = input_pre.astype(jnp.float32).reshape(shape)
    prev_f = (floor + (1.0 - floor) * jax.nn.sigmoid(prev_forget.astype(jnp.float32))).reshape(
        shape
    )
    prev_v = prev_input.astype(jnp.float32).reshape(shape)
    state = base_state
    for step in range(PROPS):
        live = (step < accepted)[:, None, None, None]
        moved = (
            prev_f[:, step][..., None] * state
            + (1.0 - prev_f[:, step])[..., None] * prev_v[:, step][:, :, None, :]
        )
        state = jnp.where(live, moved, state)
    taken_state = state
    outputs = []
    for step in range(PROPS):
        state = (
            forget[:, step][..., None] * state
            + (1.0 - forget[:, step])[..., None] * value[:, step][:, :, None, :]
        )
        outputs.append(
            jnp.einsum("bhk,bhkv->bhv", query[:, step], state, precision=lax.Precision.HIGHEST)
        )
    result = jnp.stack(outputs, axis=1)
    scaled = (
        result * lax.rsqrt(jnp.mean(result * result, axis=-1, keepdims=True) + 1e-05) * head_gain
    )
    gated = scaled * jax.nn.silu(gate_pre.astype(jnp.float32)).reshape(shape)
    mixed_heads = gated.reshape(seq_local, PROPS, head_local * HEAD_DIM).astype(jnp.bfloat16)
    own_rows = mixed_heads.shape[2]
    w_rows = lax.dynamic_slice_in_dim(w_out, lax.axis_index("tp") * own_rows, own_rows, 0)
    partial_value = jnp.dot(mixed_heads, w_rows, preferred_element_type=jnp.float32)
    finished = lax.psum(partial_value, "tp").astype(jnp.bfloat16)
    mixed = lax.all_to_all(finished, "kv", split_axis=2, concat_axis=0, tiled=True)
    return (mixed, taken_state)


def solution(mesh):
    placed = (
        P(None, None, "kv"),
        P(),
        P(None, "tp"),
        P(None, "tp"),
        P(None, "tp"),
        P(None, "tp"),
        P(),
        P("tp"),
        P(),
        P("kv", "tp", None, None),
        P("kv", None, "tp"),
        P("kv", None, "tp"),
        P("kv"),
    )
    return jax.shard_map(
        shards,
        mesh=mesh,
        in_specs=placed,
        out_specs=(P(None, None, "kv"), P("kv", "tp", None, None)),
        check_vma=False,
    )
```

profile of v0, /device:TPU:0, one launch (start us, length us, event | category | flops | bytes accessed | tf_op | source)
XLA Modules:
  0.0 96.0 jit_solution(18002514994027775703)
XLA Ops:
  0.6 7.4 %all-to-all-start = ((bf16[128,4,256]{2,1,0:T(4,128)(2,1)}), bf16[128,4,256]{2,1,0:T(4,128)(2,1)S(1)}, u32[]{:S(2)}, u32[]{:S(2)}) async-start(bf16[128,4,256]{2,1,0:T(4,128)(2,1)} %param.13), calls=%async_computation | async-start | bytes 524288 | tf_op jit(solution)/shard_map/all_to_all | solution.py:26
  8.1 0.7 broadcast_subtract_fusion.8
  8.8 0.6 copy-done.3
  9.3 0.8 multiply_add_fusion.9
  10.2 1.2 %broadcast_bitcast_fusion = f32[256]{0:T(256)} fusion(f32[128]{0:T(128)} %param.21), kind=kLoop, calls=%fused_computation.82 | loop fusion | bytes 1536 | tf_op jit(solution)/shard_map/mul | solution.py:66
  11.5 1.3 %broadcast_compare_fusion.3 = (pred[16]{0:T(512)(128)(4,1)}, pred[16]{0:T(512)(128)(4,1)}, pred[16]{0:T(512)(128)(4,1)}, pred[16]{0:T(512)(128)(4,1)}) fusion(s32[16]{0:T(128)} %param.25), kind=kLoop, calls=%fused_computation.88 | loop fusion | flops 64 | bytes 128 | tf_op jit(solution)/shard_map/gt | solution.py:48
  12.7 0.8 reshape.130
  13.5 0.6 slice_bitcast_fusion.10
  14.1 7.1 %add_select_fusion = f32[16,2,128,128]{3,2,1,0:T(8,128)S(1)} fusion(f32[16,2,128,128]{3,2,1,0:T(8,128)} %param.22, f32[16,2,128]{2,1,0:T(2,128)} %get-tuple-element.29, f32[16,2,128]{2,1,0:T(2,128)S(1)} %get-tuple-element.25, f32[16,2,128]{2,1,0:T(2,128)} %get-tuple-element.27, f32[16,2,128]{2,1,0:T(2,128)S(1)} %get-tuple-element.24, ...), kind=kLoop, calls=%fused_computation.7 | loop fusion | flops 8388608 | bytes 4390976 | tf_op jit(solution)/shard_map/jit(_where)/select_n | solution.py:53
  21.3 0.2 multiply_reduce_fusion
  21.7 1.1 %copy.38 = f32[16,4,8,256]{3,2,0,1:T(8,128)} copy(f32[16,4,8,256]{3,1,0,2:T(4,128)S(1)} %bitcast.141) | data formatting | bytes 1048576 | tf_op jit(solution)/shard_map/convert_element_type | solution.py:27
  22.8 1.9 %reshape.128 = f32[16,4,2048]{2,0,1:T(8,128)} reshape(f32[16,4,8,256]{3,2,0,1:T(8,128)} %copy.38) | data formatting | bytes 1048576 | tf_op jit(solution)/shard_map/convert_element_type | solution.py:27
  24.8 1.2 %multiply_convert_fusion = bf16[16,4,2048]{2,0,1:T(8,128)(2,1)S(1)} fusion(f32[16,4,2048]{2,0,1:T(8,128)} %reshape.128, f32[2048]{0:T(1024)S(1)} %copy-done.5, f32[16,4]{0,1:T(4,128)S(1)} %add_rsqrt_fusion.1), kind=kLoop, calls=%fused_computation.43 | loop fusion | flops 393216 | bytes 794880 | tf_op jit(solution)/shard_map/convert_element_type | solution.py:29
  25.9 1.5 %fusion.14 = f32[16,4,256]{2,0,1:T(8,128)S(1)} fusion(bf16[16,4,2048]{2,0,1:T(8,128)(2,1)S(1)} %multiply_convert_fusion, bf16[2048,256]{1,0:T(8,128)(2,1)} %param.16, f32[256]{0:T(256)S(1)} %copy-done.4, f32[256]{0:T(256)S(1)} %copy-done.2), kind=kOutput, calls=%fused_computation.21 | convolution fusion | flops 67223552 | bytes 1378304 | tf_op jit(solution)/shard_map/dot_general | solution.py:33
  27.5 1.5 %fusion.7 = f32[16,4,256]{2,0,1:T(8,128)S(1)} fusion(bf16[16,4,2048]{2,0,1:T(8,128)(2,1)S(1)} %multiply_convert_fusion, bf16[2048,256]{1,0:T(8,128)(2,1)} %param.17), kind=kOutput, calls=%fused_computation.13 | convolution fusion | flops 67141632 | bytes 1376256 | tf_op jit(solution)/shard_map/dot_general | solution.py:34
  29.1 0.7 reshape.132
  29.7 2.2 %divide_multiply_fusion = f32[16,4,256]{2,0,1:T(8,128)} fusion(bf16[16,4,2048]{2,0,1:T(8,128)(2,1)S(1)} %multiply_convert_fusion, bf16[2048,256]{1,0:T(8,128)(2,1)} %param.15), kind=kOutput, calls=%fused_computation.53 | convolution fusion | flops 67207168 | bytes 1376256 | tf_op jit(solution)/shard_map/dot_general | solution.py:32
  31.9 0.9 reshape.121
  32.8 0.8 slice_bitcast_fusion.6
  33.6 2.8 %fusion.4 = f32[16,2,1,128]{3,2,1,0:T(1,128)S(1)} fusion(f32[16,2,128,1]{2,3,1,0:T(1,128)S(1)} %bitcast.146, f32[16,2,128,128]{3,2,1,0:T(8,128)S(1)} %add_select_fusion, f32[16,2,128]{2,1,0:T(2,128)S(1)} %get-tuple-element.14, f32[16,2,128]{2,1,0:T(2,128)S(1)} %get-tuple-element.10, f32[16,2,128]{2,1,0:T(2,128)S(1)} %get-tuple-element.37), kind=kOutput, calls=%fused_computation.8 | convolution fusion | flops 7864320 | bytes 2179072 | tf_op jit(solution)/shard_map/bhk,bhkv->bhv/dot_general | solution.py:62
  36.4 4.3 %fusion.35 = f32[16,2,1,128]{3,2,1,0:T(1,128)S(1)} fusion(f32[16,2,128,1]{2,3,1,0:T(1,128)S(1)} %bitcast.155, f32[16,2,128,128]{3,2,1,0:T(8,128)S(1)} %add_select_fusion, f32[16,2,128]{2,1,0:T(2,128)S(1)} %get-tuple-element.17, f32[16,2,128]{2,1,0:T(2,128)S(1)} %get-tuple-element.13, f32[16,2,128]{2,1,0:T(2,128)S(1)} %get-tuple-element.34, ...), kind=kOutput, calls=%fused_computation.45 | convolution fusion | flops 9437184 | bytes 2228224 | tf_op jit(solution)/shard_map/bhk,bhkv->bhv/dot_general | solution.py:62
  40.7 6.1 %fusion.5 = f32[16,2,1,128]{3,2,1,0:T(1,128)S(1)} fusion(f32[16,2,128,1]{2,3,1,0:T(1,128)S(1)} %bitcast.154, f32[16,2,128]{2,1,0:T(2,128)S(1)} %get-tuple-element.16, f32[16,2,128]{2,1,0:T(2,128)S(1)} %get-tuple-element.12, f32[16,2,128]{2,1,0:T(2,128)S(1)} %get-tuple-element.35, f32[16,2,128,128]{3,2,1,0:T(8,128)S(1)} %add_select_fusion, ...), kind=kOutput, calls=%fused_computation.9 | convolution fusion | flops 11010048 | bytes 2277376 | tf_op jit(solution)/shard_map/bhk,bhkv->bhv/dot_general | solution.py:62
  46.8 7.2 %fusion = f32[16,2,1,128]{3,2,1,0:T(1,128)S(1)} fusion(f32[16,2,128,1]{2,3,1,0:T(1,128)S(1)} %bitcast.153, f32[16,2,128]{2,1,0:T(2,128)S(1)} %get-tuple-element.15, f32[16,2,128]{2,1,0:T(2,128)S(1)} %get-tuple-element.11, f32[16,2,128]{2,1,0:T(2,128)S(1)} %get-tuple-element.36, f32[16,2,128]{2,1,0:T(2,128)S(1)} %get-tuple-element.16, ...), kind=kOutput, calls=%fused_computation | convolution fusion | flops 12582912 | bytes 2326528 | tf_op jit(solution)/shard_map/bhk,bhkv->bhv/dot_general | solution.py:62
  54.1 0.1 fusion.39
  54.2 0.1 mul.343
  54.4 2.0 %fusion.16 = f32[16,4,2048]{2,0,1:T(8,128)S(1)} fusion(bf16[1024,2048]{1,0:T(8,128)(2,1)} %param.19, s32[]{:T(128)S(6)} %select_n.20, f32[16,4,256]{2,0,1:T(8,128)S(1)} %mul.344, f32[16,1,256]{2,0,1:T(8,128)S(1)} %stack.28, f32[16,1,256]{2,0,1:T(8,128)S(1)} %stack.27, f32[16,1,256]{2,0,1:T(8,128)S(1)} %stack.26, f32[16,1,256]{2,0,1:T(8,128)S(1)} %stack.25, ...), kind=kOutput, calls=%fused_computation.24 | convolution fusion | flops 134430720 | bytes 3015684 | tf_op jit(solution)/shard_map/dot_general | solution.py:72
  56.5 16.6 %all-reduce.1 = bf16[16,4,2048]{2,0,1:T(8,128)(2,1)S(1)} all-reduce(f32[16,4,2048]{2,0,1:T(8,128)S(1)} %fusion.16), channel_id=1, replica_groups=mesh['kv'=8,'tp'=4] {'tp'}, use_global_device_ids=true, to_apply=%region_3.4 | all-reduce | flops 131072 | bytes 786432 | tf_op jit(solution)/shard_map/psum | solution.py:73
  73.1 1.4 %copy.45 = bf16[16,4,2048]{0,1,2:T(4,128)(2,1)S(1)} copy(bf16[16,4,2048]{2,0,1:T(8,128)(2,1)S(1)} %all-reduce.1) | data formatting | bytes 524288 | tf_op jit(solution)/shard_map/convert_element_type | solution.py:73
  74.5 2.2 %reshape.148 = bf16[8,2,8192]{2,1,0:T(2,128)(2,1)S(1)} reshape(bf16[2048,4,16]{2,1,0:T(4,128)(2,1)S(1)} %bitcast.139) | data formatting | bytes 524288
  76.7 14.9 %all_to_all.27 = bf16[8,2,8192]{2,1,0:T(2,128)(2,1)} all-to-all(bf16[8,2,8192]{2,1,0:T(2,128)(2,1)S(1)} %reshape.148), channel_id=1, replica_groups=mesh['kv'=8,'tp'=4] {'kv'}, dimensions={0} | all-to-all | bytes 524288 | tf_op jit(solution)/shard_map/all_to_all | solution.py:74
  91.5 2.4 %reshape.149 = bf16[2048,4,16]{2,1,0:T(4,128)(2,1)S(1)} reshape(bf16[8,2,8192]{2,1,0:T(2,128)(2,1)} %all_to_all.27) | data formatting | bytes 524288
  94.0 2.0 %copy.46 = bf16[8,16,4,256]{3,2,1,0:T(4,128)(2,1)} copy(bf16[8,16,4,256]{1,2,3,0:T(4,128)(2,1)S(1)} %bitcast.140) | data formatting | bytes 524288 | tf_op jit(solution)/shard_map/all_to_all | solution.py:74
  (30 shorter events, 0.5 us)
Async XLA Ops:
  0.6 53.8 %copy-start = (bf16[2048,256]{1,0:T(8,128)(2,1)S(1)}, bf16[2048,256]{1,0:T(8,128)(2,1)}, u32[]{:S(2)}) copy-start(bf16[2048,256]{1,0:T(8,128)(2,1)} %param.18) | copy-start | bytes 3145732
  0.6 20.7 %all-to-all-start = ((bf16[128,4,256]{2,1,0:T(4,128)(2,1)}), bf16[128,4,256]{2,1,0:T(4,128)(2,1)S(1)}, u32[]{:S(2)}, u32[]{:S(2)}) async-start(bf16[128,4,256]{2,1,0:T(4,128)(2,1)} %param.13), calls=%async_computation | async-start | bytes 524288 | tf_op jit(solution)/shard_map/all_to_all | solution.py:26
  8.8 0.6 copy-start.3
  21.3 25.5 %copy-start.1 = (f32[16,2,128,128]{3,2,1,0:T(8,128)}, f32[16,2,128,128]{3,2,1,0:T(8,128)S(1)}, u32[]{:S(2)}) copy-start(f32[16,2,128,128]{3,2,1,0:T(8,128)S(1)} %add_select_fusion) | copy-start | bytes 6291460
  21.3 3.5 %copy-start.5 = (f32[2048]{0:T(1024)S(1)}, f32[2048]{0:T(1024)}, u32[]{:S(2)}) copy-start(f32[2048]{0:T(1024)} %param.14) | copy-start | bytes 24580
  21.3 4.6 %copy-start.2 = (f32[256]{0:T(256)S(1)}, f32[256]{0:T(256)}, u32[]{:S(2)}) copy-start(f32[256]{0:T(256)} %param.20) | copy-start | bytes 3076
  21.3 4.6 %copy-start.4 = (f32[256]{0:T(256)S(1)}, f32[256]{0:T(256)}, u32[]{:S(2)}) copy-start(f32[256]{0:T(256)} %copy-done.3) | copy-start | bytes 3076
  46.8 7.7 %copy-start.6 = (f32[256]{0:T(256)S(1)}, f32[256]{0:T(256)}, u32[]{:S(2)}) copy-start(f32[256]{0:T(256)} %broadcast_bitcast_fusion) | copy-start | bytes 3076
where the time goes:
time: 96.9 us; the launch traced here: 96 us
  blocking collectives  31.5 us (33%)
  matrix products  27.6 us (28%)
  local copies, waits for them, and re-layouts  17 us (18%)
  other arithmetic  11.5 us (12%)
  starting transfers between devices  7.42 us (8%)
    dot_general x4, matrix products, shards(): jnp.einsum('bhk,bhkv->bhv', query[:, step], state, precision=lax.Precisio...  20.3 us
    psum x1, blocking collectives, shards(): finished = lax.psum(partial_value, 'tp').astype(jnp.bfloat16)  16.6 us
    all_to_all x1, blocking collectives, shards(): lax.all_to_all(finished, 'kv', split_axis=2, concat_axis=0, tiled=True)  14.9 us
    all_to_all x1, starting transfers between devices, shards(): lax.all_to_all(hidden, 'kv', split_axis=0, concat_axis=2, tiled=True)  7.42 us
    select_n x1, other arithmetic, shards(): state = jnp.where(live, moved, state)  7.13 us
    unnamed x17, local copies, waits for them, and re-layouts  5.27 us
    convert_element_type x2, local copies, waits for them, and re-layouts, shards(): whole_vals = arrived.astype(jnp.float32)  3.03 us
    dot_general x1, matrix products, shards(): jnp.dot(normed, w_query, preferred_element_type=jnp.float32)  2.17 us
  transfers between devices with their start and end apart: 1, of which 0 were waited for; matrix products, arithmetic and copies ran while one was open for 13% of the time, Pallas kernels for 0%

commit v1 on v0

--- a/solution.py
+++ b/solution.py
@@ -71,7 +71,20 @@
     w_rows = lax.dynamic_slice_in_dim(w_out, lax.axis_index("tp") * own_rows, own_rows, 0)
     partial_value = jnp.dot(mixed_heads, w_rows, preferred_element_type=jnp.float32)
     finished = lax.psum(partial_value, "tp").astype(jnp.bfloat16)
-    mixed = lax.all_to_all(finished, "kv", split_axis=2, concat_axis=0, tiled=True)
+
+    def desk_feed(work_x, a_name):
+        right_arr = jnp.concatenate(
+            lax.all_to_all(
+                jnp.stack(jnp.split(work_x, lax.axis_size(a_name), 2), 0),
+                axis_name=a_name,
+                split_axis=0,
+                concat_axis=0,
+            ),
+            0,
+        )
+        return right_arr
+
+    mixed = desk_feed(finished, "kv")
     return (mixed, taken_state)
 
 

time: 96.9 us -> 89.9 us (0.928)
  local copies, waits for them, and re-layouts: 17 us -> 10 us
    unnamed x17 -> x23, local copies, waits for them, and re-layouts: 5.27 us -> 1.64 us
    all_to_all x1, local copies, waits for them, and re-layouts: 2.02 us -> 0.02 us  [desk_feed(): lax.all_to_all(jnp.stack(jnp.split(work_x, lax.axis_size(a_name), 2), 0),...]
    convert_element_type x1 -> x0, local copies, waits for them, and re-layouts: 1.36 us -> none  [shards(): finished = lax.psum(partial_value, 'tp').astype(jnp.bfloat16)]
  transfers between devices with their start and end apart: 1 -> 1, of which waited for: 0 -> 0; matrix products, arithmetic and copies ran while one was open for 13% -> 14% of each run, Pallas kernels for 0% -> 0%
where the time goes in v1:
time: 89.9 us; the launch traced here: 88.9 us
  blocking collectives  31.4 us (35%)
  matrix products  27.6 us (31%)
  other arithmetic  11.5 us (13%)
  local copies, waits for them, and re-layouts  10 us (11%)
  starting transfers between devices  7.42 us (8%)
  between operations  0.98 us (1%)
    dot_general x4, matrix products, shards(): jnp.einsum('bhk,bhkv->bhv', query[:, step], state, precision=lax.Precisio...  20.3 us
    psum x1, blocking collectives, shards(): finished = lax.psum(partial_value, 'tp').astype(jnp.bfloat16)  16.6 us
    all_to_all x1, blocking collectives, desk_feed(): lax.all_to_all(jnp.stack(jnp.split(work_x, lax.axis_size(a_name), 2), 0),...  14.7 us
    all_to_all x1, starting transfers between devices, shards(): lax.all_to_all(hidden, 'kv', split_axis=0, concat_axis=2, tiled=True)  7.42 us
    select_n x1, other arithmetic, shards(): state = jnp.where(live, moved, state)  7.13 us
    convert_element_type x2, local copies, waits for them, and re-layouts, shards(): whole_vals = arrived.astype(jnp.float32)  3.03 us
    dot_general x1, matrix products, shards(): jnp.dot(normed, w_query, preferred_element_type=jnp.float32)  2.17 us
    dot_general x1, matrix products, shards(): jnp.dot(mixed_heads, w_rows, preferred_element_type=jnp.float32)  2.04 us
  transfers between devices with their start and end apart: 1, of which 0 were waited for; matrix products, arithmetic and copies ran while one was open for 14% of the time, Pallas kernels for 0%

profile of v1, /device:TPU:0, one launch (start us, length us, event | category | flops | bytes accessed | tf_op | source)
XLA Modules:
  0.0 88.9 jit_solution(12442321354526438328)
XLA Ops:
  0.6 7.4 %all-to-all-start = ((bf16[128,4,256]{2,1,0:T(4,128)(2,1)}), bf16[128,4,256]{2,1,0:T(4,128)(2,1)S(1)}, u32[]{:S(2)}, u32[]{:S(2)}) async-start(bf16[128,4,256]{2,1,0:T(4,128)(2,1)} %param.13), calls=%async_computation | async-start | bytes 524288 | tf_op jit(solution)/shard_map/all_to_all | solution.py:26
  8.1 0.7 broadcast_subtract_fusion.8
  8.8 0.6 copy-done.3
  9.3 0.8 multiply_add_fusion.9
  10.2 1.2 %broadcast_bitcast_fusion = f32[256]{0:T(256)} fusion(f32[128]{0:T(128)} %param.21), kind=kLoop, calls=%fused_computation.98 | loop fusion | bytes 1536 | tf_op jit(solution)/shard_map/mul | solution.py:66
  11.5 1.3 %broadcast_compare_fusion.3 = (pred[16]{0:T(512)(128)(4,1)}, pred[16]{0:T(512)(128)(4,1)}, pred[16]{0:T(512)(128)(4,1)}, pred[16]{0:T(512)(128)(4,1)}) fusion(s32[16]{0:T(128)} %param.25), kind=kLoop, calls=%fused_computation.104 | loop fusion | flops 64 | bytes 128 | tf_op jit(solution)/shard_map/gt | solution.py:48
  12.7 0.8 reshape.134
  13.5 0.6 slice_bitcast_fusion.18
  14.1 7.1 %add_select_fusion = f32[16,2,128,128]{3,2,1,0:T(8,128)S(1)} fusion(f32[16,2,128,128]{3,2,1,0:T(8,128)} %param.22, f32[16,2,128]{2,1,0:T(2,128)} %get-tuple-element.35, f32[16,2,128]{2,1,0:T(2,128)S(1)} %get-tuple-element.31, f32[16,2,128]{2,1,0:T(2,128)} %get-tuple-element.33, f32[16,2,128]{2,1,0:T(2,128)S(1)} %get-tuple-element.30, ...), kind=kLoop, calls=%fused_computation.7 | loop fusion | flops 8388608 | bytes 4390976 | tf_op jit(solution)/shard_map/jit(_where)/select_n | solution.py:53
  21.3 0.2 multiply_reduce_fusion
  21.6 0.1 copy.54
  21.7 0.1 convert_element_type.70
  21.7 1.1 %copy.37 = f32[16,4,8,256]{3,2,0,1:T(8,128)} copy(f32[16,4,8,256]{3,1,0,2:T(4,128)S(1)} %bitcast.166) | data formatting | bytes 1048576 | tf_op jit(solution)/shard_map/convert_element_type | solution.py:27
  22.8 1.9 %reshape.132 = f32[16,4,2048]{2,0,1:T(8,128)} reshape(f32[16,4,8,256]{3,2,0,1:T(8,128)} %copy.37) | data formatting | bytes 1048576 | tf_op jit(solution)/shard_map/convert_element_type | solution.py:27
  24.8 1.2 %multiply_convert_fusion = bf16[16,4,2048]{2,0,1:T(8,128)(2,1)S(1)} fusion(f32[16,4,2048]{2,0,1:T(8,128)} %reshape.132, f32[2048]{0:T(1024)S(1)} %copy-done.5, f32[16,4]{0,1:T(4,128)S(1)} %add_rsqrt_fusion.1), kind=kLoop, calls=%fused_computation.43 | loop fusion | flops 393216 | bytes 794880 | tf_op jit(solution)/shard_map/convert_element_type | solution.py:29
  25.9 1.5 %fusion.14 = f32[16,4,256]{2,0,1:T(8,128)S(1)} fusion(bf16[16,4,2048]{2,0,1:T(8,128)(2,1)S(1)} %multiply_convert_fusion, bf16[2048,256]{1,0:T(8,128)(2,1)} %param.16, f32[256]{0:T(256)S(1)} %copy-done.4, f32[256]{0:T(256)S(1)} %copy-done.2), kind=kOutput, calls=%fused_computation.21 | convolution fusion | flops 67223552 | bytes 1378304 | tf_op jit(solution)/shard_map/dot_general | solution.py:33
  27.5 1.5 %fusion.7 = f32[16,4,256]{2,0,1:T(8,128)S(1)} fusion(bf16[16,4,2048]{2,0,1:T(8,128)(2,1)S(1)} %multiply_convert_fusion, bf16[2048,256]{1,0:T(8,128)(2,1)} %param.17), kind=kOutput, calls=%fused_computation.13 | convolution fusion | flops 67141632 | bytes 1376256 | tf_op jit(solution)/shard_map/dot_general | solution.py:34
  29.1 0.7 reshape.136
  29.7 2.2 %divide_multiply_fusion = f32[16,4,256]{2,0,1:T(8,128)} fusion(bf16[16,4,2048]{2,0,1:T(8,128)(2,1)S(1)} %multiply_convert_fusion, bf16[2048,256]{1,0:T(8,128)(2,1)} %param.15), kind=kOutput, calls=%fused_computation.53 | convolution fusion | flops 67207168 | bytes 1376256 | tf_op jit(solution)/shard_map/dot_general | solution.py:32
  31.9 0.9 reshape.124
  32.8 0.8 slice_bitcast_fusion.14
  33.6 2.8 %fusion.4 = f32[16,2,1,128]{3,2,1,0:T(1,128)S(1)} fusion(f32[16,2,128,1]{2,3,1,0:T(1,128)S(1)} %bitcast.171, f32[16,2,128,128]{3,2,1,0:T(8,128)S(1)} %add_select_fusion, f32[16,2,128]{2,1,0:T(2,128)S(1)} %get-tuple-element.20, f32[16,2,128]{2,1,0:T(2,128)S(1)} %get-tuple-element.16, f32[16,2,128]{2,1,0:T(2,128)S(1)} %get-tuple-element.43), kind=kOutput, calls=%fused_computation.8 | convolution fusion | flops 7864320 | bytes 2179072 | tf_op jit(solution)/shard_map/bhk,bhkv->bhv/dot_general | solution.py:62
  36.4 4.3 %fusion.35 = f32[16,2,1,128]{3,2,1,0:T(1,128)S(1)} fusion(f32[16,2,128,1]{2,3,1,0:T(1,128)S(1)} %bitcast.180, f32[16,2,128,128]{3,2,1,0:T(8,128)S(1)} %add_select_fusion, f32[16,2,128]{2,1,0:T(2,128)S(1)} %get-tuple-element.23, f32[16,2,128]{2,1,0:T(2,128)S(1)} %get-tuple-element.19, f32[16,2,128]{2,1,0:T(2,128)S(1)} %get-tuple-element.40, ...), kind=kOutput, calls=%fused_computation.45 | convolution fusion | flops 9437184 | bytes 2228224 | tf_op jit(solution)/shard_map/bhk,bhkv->bhv/dot_general | solution.py:62
  40.7 6.1 %fusion.5 = f32[16,2,1,128]{3,2,1,0:T(1,128)S(1)} fusion(f32[16,2,128,1]{2,3,1,0:T(1,128)S(1)} %bitcast.179, f32[16,2,128]{2,1,0:T(2,128)S(1)} %get-tuple-element.22, f32[16,2,128]{2,1,0:T(2,128)S(1)} %get-tuple-element.18, f32[16,2,128]{2,1,0:T(2,128)S(1)} %get-tuple-element.41, f32[16,2,128,128]{3,2,1,0:T(8,128)S(1)} %add_select_fusion, ...), kind=kOutput, calls=%fused_computation.9 | convolution fusion | flops 11010048 | bytes 2277376 | tf_op jit(solution)/shard_map/bhk,bhkv->bhv/dot_general | solution.py:62
  46.8 7.2 %fusion = f32[16,2,1,128]{3,2,1,0:T(1,128)S(1)} fusion(f32[16,2,128,1]{2,3,1,0:T(1,128)S(1)} %bitcast.178, f32[16,2,128]{2,1,0:T(2,128)S(1)} %get-tuple-element.21, f32[16,2,128]{2,1,0:T(2,128)S(1)} %get-tuple-element.17, f32[16,2,128]{2,1,0:T(2,128)S(1)} %get-tuple-element.42, f32[16,2,128]{2,1,0:T(2,128)S(1)} %get-tuple-element.22, ...), kind=kOutput, calls=%fused_computation | convolution fusion | flops 12582912 | bytes 2326528 | tf_op jit(solution)/shard_map/bhk,bhkv->bhv/dot_general | solution.py:62
  54.1 0.1 fusion.39
  54.2 0.1 mul.343
  54.4 0.1 mul.344
  54.4 2.0 %fusion.16 = f32[16,4,2048]{2,0,1:T(8,128)S(1)} fusion(bf16[1024,2048]{1,0:T(8,128)(2,1)} %param.19, s32[]{:T(128)S(6)} %select_n.20, f32[16,4,256]{2,0,1:T(8,128)S(1)} %mul.344, f32[16,1,256]{2,0,1:T(8,128)S(1)} %stack.55, f32[16,1,256]{2,0,1:T(8,128)S(1)} %stack.54, f32[16,1,256]{2,0,1:T(8,128)S(1)} %stack.53, f32[16,1,256]{2,0,1:T(8,128)S(1)} %stack.52, ...), kind=kOutput, calls=%fused_computation.24 | convolution fusion | flops 134430720 | bytes 3015684 | tf_op jit(solution)/shard_map/dot_general | solution.py:72
  56.5 16.6 %all-reduce.1 = bf16[16,4,2048]{2,0,1:T(8,128)(2,1)S(1)} all-reduce(f32[16,4,2048]{2,0,1:T(8,128)S(1)} %fusion.16), channel_id=1, replica_groups=mesh['kv'=8,'tp'=4] {'tp'}, use_global_device_ids=true, to_apply=%region_3.4 | all-reduce | flops 131072 | bytes 786432 | tf_op jit(solution)/shard_map/psum | solution.py:73
  73.3 14.7 %all_to_all.14 = bf16[8,16,4,256]{3,1,2,0:T(8,128)(2,1)S(1)} all-to-all(bf16[8,16,4,256]{3,1,2,0:T(8,128)(2,1)S(1)} %fusion.46), channel_id=1, replica_groups=mesh['kv'=8,'tp'=4] {'kv'}, dimensions={0} | all-to-all | bytes 524288 | tf_op jit(solution)/shard_map/all_to_all | solution.py:77
  88.0 0.9 %copy.45 = bf16[128,4,256]{2,1,0:T(4,128)(2,1)} copy(bf16[128,4,256]{2,0,1:T(8,128)(2,1)S(1)} %bitcast.167) | data formatting | bytes 524288
  (36 shorter events, 0.4 us)
Async XLA Ops:
  0.6 53.8 %copy-start = (bf16[2048,256]{1,0:T(8,128)(2,1)S(1)}, bf16[2048,256]{1,0:T(8,128)(2,1)}, u32[]{:S(2)}) copy-start(bf16[2048,256]{1,0:T(8,128)(2,1)} %param.18) | copy-start | bytes 3145732
  0.6 20.7 %all-to-all-start = ((bf16[128,4,256]{2,1,0:T(4,128)(2,1)}), bf16[128,4,256]{2,1,0:T(4,128)(2,1)S(1)}, u32[]{:S(2)}, u32[]{:S(2)}) async-start(bf16[128,4,256]{2,1,0:T(4,128)(2,1)} %param.13), calls=%async_computation | async-start | bytes 524288 | tf_op jit(solution)/shard_map/all_to_all | solution.py:26
  8.8 0.6 copy-start.3
  21.3 25.5 %copy-start.1 = (f32[16,2,128,128]{3,2,1,0:T(8,128)}, f32[16,2,128,128]{3,2,1,0:T(8,128)S(1)}, u32[]{:S(2)}) copy-start(f32[16,2,128,128]{3,2,1,0:T(8,128)S(1)} %add_select_fusion) | copy-start | bytes 6291460
  21.3 3.5 %copy-start.5 = (f32[2048]{0:T(1024)S(1)}, f32[2048]{0:T(1024)}, u32[]{:S(2)}) copy-start(f32[2048]{0:T(1024)} %param.14) | copy-start | bytes 24580
  21.3 4.6 %copy-start.2 = (f32[256]{0:T(256)S(1)}, f32[256]{0:T(256)}, u32[]{:S(2)}) copy-start(f32[256]{0:T(256)} %param.20) | copy-start | bytes 3076
  21.3 4.6 %copy-start.4 = (f32[256]{0:T(256)S(1)}, f32[256]{0:T(256)}, u32[]{:S(2)}) copy-start(f32[256]{0:T(256)} %copy-done.3) | copy-start | bytes 3076
  46.8 7.7 %copy-start.6 = (f32[256]{0:T(256)S(1)}, f32[256]{0:T(256)}, u32[]{:S(2)}) copy-start(f32[256]{0:T(256)} %broadcast_bitcast_fusion) | copy-start | bytes 3076
